TPU v7x, 256 devices: a whole 4x4x8 slice. The times are simulated.
256 devices in a mesh: sp: 64 (over z, x, core), tp: 4 (over y).
Axes of the slice: x: 4, y: 4, z: 8, core: 2. Of those that a mesh axis runs over, the one named last changes fastest.
Arguments:
- inputs: bfloat16 [40960, 2048], P('sp', 'tp'), may hold values from -6 to 6
- norm_gain: bfloat16 [2048], P('tp'), may hold values from 0.099609375 to 1.8984375
- query_weight: bfloat16 [2048, 2048], P('sp', 'tp'), may hold values from -0.125 to 0.125
- key_weight: bfloat16 [2048, 2048], P('sp', 'tp'), may hold values from -0.125 to 0.125
- value_weight: bfloat16 [2048, 2048], P('sp', 'tp'), may hold values from -0.125 to 0.125
- outgate_weight: bfloat16 [2048, 2048], P('sp', 'tp'), may hold values from -0.125 to 0.125
- inputgate_weight: bfloat16 [2048, 8], replicated, may hold values from -1 to 1
- forget_weight: bfloat16 [2048, 8], replicated, may hold values from -0.125 to 0.125
- forget_bias: float32 [8], P('tp'), may hold values from -1.1 to 2.25
- conv_query: float32 [4, 2048], P(None, 'tp'), may hold values from -3 to 3
- conv_key: float32 [4, 2048], P(None, 'tp'), may hold values from -3 to 3
- cell_gain: float32 [2048], P('tp'), may hold values from 0.1 to 1.9
- pool_weight: bfloat16 [2048, 1024], P('sp', 'tp'), may hold values from -0.125 to 0.125
- group_weight: bfloat16 [8, 128, 128], P('tp'), may hold values from -0.5 to 0.5
- pool_gain: float32 [1024], P('tp'), may hold values from 0.1 to 1.9
- cell_out_weight: bfloat16 [2048, 2048], P('tp', 'sp'), may hold values from -0.109375 to 0.109375
- pool_out_weight: bfloat16 [1024, 2048], P('tp', 'sp'), may hold values from -0.109375 to 0.109375
Outputs:
- mixed: bfloat16 [40960, 2048], P(('sp', 'tp'))
All inputs are finite; a program needn't handle non-finite values.
Results may differ from a plain program's by a relative error of at most 0.013.
The roundings to bfloat16 on the way count: a program that leaves them out, or rounds other values in their place, can miss the bound.
Values may be sent and summed in bfloat16 or wider, within the bound.
A program may use at most 128 MiB of HBM per device.

v0:
```python
import math

import jax
import jax.numpy as jnp
from jax import lax
from jax.sharding import Mesh
from jax.sharding import PartitionSpec as P

LEVELS = 4
SP = ("sp_0", "sp_1", "sp_2")
SP_TP = ("sp_0", "sp_1", "sp_2", "tp")


epsilon = 1e-06
big_negative = -1e30
highest = lax.Precision.HIGHEST


def copy_for_each(array, axis):
    copies = jnp.broadcast_to(array, (lax.axis_size(axis), *array.shape))
    return lax.all_to_all(copies, axis, split_axis=0, concat_axis=0, tiled=True)


def taken_together(array, axis):
    everything = copy_for_each(array, axis)
    return jnp.sum(everything, axis=0)


def joined_along(pieces, dim):
    dims = list(pieces.shape[1:])
    dims[dim] *= pieces.shape[0]
    return jnp.moveaxis(pieces, 0, dim).reshape(dims)


def gather_directly(array, axis, dim):
    pieces = copy_for_each(array, axis)
    return joined_along(pieces, dim)


def in_one_piece(arrays, axis, dim, along):
    both = jnp.concatenate(arrays, axis=along)
    result, at, done = (lax.all_gather(both, axis, axis=dim, tiled=True), 0, [])
    for a in arrays:
        done.append(lax.slice_in_dim(result, at, at + a.shape[along], axis=along))
        at += a.shape[along]
    return tuple(done)


def shifted(block, axis, distance):
    devices = range(lax.axis_size(axis))
    route = [(i - distance, i) for i in devices if i - distance in devices]
    return lax.ppermute(block, axis, route)


def nothing_yet(array, identity):
    return jax.tree.map(
        lambda part, zero: jnp.zeros_like(part) + jnp.asarray(zero, part.dtype), array, identity
    )


def collected_together(array, axis):
    leaves = jax.tree.leaves(array)
    turns = sorted(range(len(leaves)), key=lambda k: -leaves[k].size)
    width = (1, *leaves[turns[0]].shape)[-1]
    lines = [
        jnp.pad(leaves[k].reshape(-1), (0, -leaves[k].size % width)).reshape(-1, width)
        for k in turns
    ]
    both, at, found = (lax.all_gather(jnp.concatenate(lines), axis), 0, {})
    for k, line in zip(turns, lines):
        slab = both[:, at : at + len(line)].reshape(len(both), -1)
        found[k] = slab[:, : leaves[k].size].reshape(-1, *leaves[k].shape)
        at += len(line)
    numbers = iter(range(len(leaves)))
    return jax.tree.map(lambda _: found[next(numbers)], array)


def carried_in(array, axes, combine, identity):
    before = start = nothing_yet(array, identity)
    subtotal = array
    for axis in reversed(axes):
        count, place = (lax.axis_size(axis), lax.axis_index(axis))
        pieces = collected_together(subtotal, axis)
        inside, subtotal = (start, start)
        for k in range(count):
            passed = k < place
            subtotal = combine(subtotal, jax.tree.map(lambda part: part[k], pieces))
            inside = jax.tree.map(lambda new, old: jnp.where(passed, new, old), subtotal, inside)
        before = combine(inside, before)
    return before


def rows_first(arrays, axis, dims):
    turned = [jnp.moveaxis(a, dim, 0) for a, dim in zip(arrays, dims)]
    both = jnp.concatenate([t.reshape(len(t), -1) for t in turned], axis=1)
    result, at, done = (lax.all_gather(both, axis, axis=0, tiled=True), 0, [])
    for t, dim in zip(turned, dims):
        slab = result[:, at : at + t[0].size].reshape(-1, *t.shape[1:])
        done.append(jnp.moveaxis(slab, 0, dim))
        at += t[0].size
    return tuple(done)


def cut_along(array, dim, count):
    dims = array.shape
    pieces = array.reshape(*dims[:dim], count, dims[dim] // count, *dims[dim + 1 :])
    return jnp.moveaxis(pieces, dim, 0)


def summed_on_arrival(array, axis, dim):
    count = lax.axis_size(axis)
    pieces = lax.all_to_all(cut_along(array, dim, count), axis, 0, 0, tiled=True)
    return jnp.sum(pieces.astype(jnp.float32), axis=0)


def causal_taps(padded, taps):
    span_rows = padded.shape[0] - taps.shape[0] + 1
    running = jnp.zeros((span_rows, padded.shape[1]), jnp.float32)
    for lag_index in range(taps.shape[0]):
        running = running + taps[lag_index] * padded[lag_index : lag_index + span_rows].astype(
            jnp.float32
        )
    return running


def combine_states(earlier, later):
    memory_early, normal_early, ceiling_early, fall_early = earlier
    memory_late, normal_late, ceiling_late, fall_late = later
    ceiling = jnp.maximum(fall_late + ceiling_early, ceiling_late)
    left_weight = jnp.exp(fall_late + ceiling_early - ceiling)
    right_weight = jnp.exp(ceiling_late - ceiling)
    memory = left_weight[:, None, None] * memory_early + right_weight[:, None, None] * memory_late
    normal = left_weight[:, None] * normal_early + right_weight[:, None] * normal_late
    return (memory, normal, ceiling, fall_early + fall_late)


def cell_outputs(queries, key_rows, value_rows, log_in, cumulative, memory, normalizer, stabilizer):
    length = queries.shape[0]
    query_wide = queries.astype(jnp.float32)
    cum_heads = cumulative.T
    in_heads = log_in.T
    causal = jnp.arange(length)[:, None] >= jnp.arange(length)[None, :]
    decay_log = cum_heads[:, :, None] - cum_heads[:, None, :] + in_heads[:, None, :]
    decay_log = jnp.where(causal[None, :, :], decay_log, -jnp.inf)
    carried_log = cum_heads + stabilizer[:, None]
    ceiling = jnp.maximum(carried_log, jnp.max(decay_log, axis=2))
    within = jnp.exp(decay_log - ceiling[:, :, None])
    carried = jnp.exp(carried_log - ceiling)
    raw_scores = jnp.einsum("thd,shd->hts", queries, key_rows, preferred_element_type=jnp.float32)
    scores = (raw_scores * within).astype(jnp.bfloat16)
    numerator = carried.T[:, :, None] * jnp.einsum(
        "hvk,thk->thv", memory, query_wide, precision=highest
    )
    numerator = numerator + jnp.einsum(
        "hts,shv->thv", scores, value_rows, preferred_element_type=jnp.float32
    )
    denominator = (
        carried.T * jnp.einsum("hk,thk->th", normalizer, query_wide, precision=highest)
        + jnp.sum(scores.astype(jnp.float32), axis=2).T
    )
    return numerator / jnp.maximum(jnp.abs(denominator), jnp.exp(-ceiling.T))[:, :, None]


def local(
    inputs,
    norm_gain,
    query_weight,
    key_weight,
    value_weight,
    outgate_weight,
    inputgate_weight,
    forget_weight,
    forget_bias,
    conv_query,
    conv_key,
    cell_gain,
    pool_weight,
    group_weight,
    pool_gain,
    cell_out_weight,
    pool_out_weight,
):
    local_wide = inputs.astype(jnp.float32)
    squares = taken_together(jnp.sum(local_wide * local_wide, axis=1, keepdims=True), "tp")
    normed = gather_directly(
        (local_wide * norm_gain.astype(jnp.float32)).astype(jnp.bfloat16), "tp", 1
    )
    inverse_rms = lax.rsqrt(squares / normed.shape[1] + epsilon)
    pieces = in_one_piece(
        (query_weight, key_weight, value_weight, outgate_weight, pool_weight), SP, 0, 1
    )
    products = tuple(
        (jnp.dot(normed, piece_rows, preferred_element_type=jnp.float32) for piece_rows in pieces)
    )
    query_pre, key_pre, value_rows, outgate_pre, pool_pre = tuple(
        ((product * inverse_rms).astype(jnp.bfloat16) for product in products)
    )
    tp_index = lax.axis_index("tp")
    sp_index = lax.axis_index(SP)
    tokens_here = inputs.shape[0]
    sequence_log = math.log(tokens_here * lax.axis_size(SP))
    local_heads = forget_bias.shape[0]
    gate_cols = lax.dynamic_slice_in_dim(inputgate_weight, tp_index * local_heads, local_heads, 1)
    keep_cols = lax.dynamic_slice_in_dim(forget_weight, tp_index * local_heads, local_heads, 1)
    log_in = jnp.dot(normed, gate_cols, preferred_element_type=jnp.float32) * inverse_rms
    log_keep = jax.nn.log_sigmoid(
        jnp.dot(normed, keep_cols, preferred_element_type=jnp.float32) * inverse_rms
        + forget_bias
        + sequence_log
    )
    widest = 2**LEVELS - 1
    query_width = query_pre.shape[1]
    edges = jnp.concatenate([query_pre[-widest:], key_pre[-widest:], pool_pre[-widest:]], axis=1)
    before = shifted(edges, SP, 1)
    margin = conv_query.shape[0] - 1
    query_taps = causal_taps(
        jnp.concatenate([before[widest - margin :, :query_width], query_pre], axis=0), conv_query
    )
    key_taps = causal_taps(
        jnp.concatenate(
            [before[widest - margin :, query_width : 2 * query_width], key_pre], axis=0
        ),
        conv_key,
    )
    pool_before = before[:, 2 * query_width :]
    head_size = query_width // local_heads
    queries = (
        (jax.nn.silu(query_taps) * head_size ** (-0.5))
        .astype(jnp.bfloat16)
        .reshape(tokens_here, local_heads, head_size)
    )
    key_rows = (
        jax.nn.silu(key_taps).astype(jnp.bfloat16).reshape(tokens_here, local_heads, head_size)
    )
    value_heads = value_rows.reshape(tokens_here, local_heads, head_size)
    key_wide = key_rows.astype(jnp.float32)
    cumulative = jnp.cumsum(log_keep, axis=0)
    final_log = cumulative[-1]
    lead_log = final_log[None, :] - cumulative + log_in
    own_ceiling = jnp.max(lead_log, axis=0)
    share_weight = jnp.exp(lead_log - own_ceiling[None, :])
    weighted = (value_heads.astype(jnp.float32) * share_weight[:, :, None]).astype(jnp.bfloat16)
    own_memory = jnp.einsum("shv,shk->hvk", weighted, key_rows, preferred_element_type=jnp.float32)
    own_normalizer = jnp.einsum("sh,shk->hk", share_weight, key_wide, precision=highest)
    identity = (
        jnp.zeros_like(own_memory),
        jnp.zeros_like(own_normalizer),
        jnp.full_like(own_ceiling, big_negative),
        jnp.zeros_like(final_log),
    )
    memory_in, normalizer_in, ceiling_in, fall_in = carried_in(
        (own_memory, own_normalizer, own_ceiling, final_log), SP, combine_states, identity
    )
    hidden = cell_outputs(
        queries, key_rows, value_heads, log_in, cumulative, memory_in, normalizer_in, ceiling_in
    )
    normalized = hidden * lax.rsqrt(jnp.mean(hidden * hidden, axis=2, keepdims=True) + epsilon)
    cell_mix = (
        normalized.reshape(tokens_here, query_width)
        * cell_gain
        * jax.nn.sigmoid(outgate_pre.astype(jnp.float32))
    ).astype(jnp.bfloat16)
    local_groups = group_weight.shape[0]
    group_width = pool_pre.shape[1] // local_groups
    group_ids = tp_index * local_groups + jnp.arange(local_groups, dtype=jnp.int32)
    reach_rows = 2 ** (1 + group_ids % LEVELS)
    row_ids = jnp.arange(tokens_here, dtype=jnp.int32)
    column_ids = jnp.arange(tokens_here + widest, dtype=jnp.int32)
    distance = row_ids[:, None] + widest - column_ids[None, :]
    band = (
        (distance[None, :, :] >= 0) & (distance[None, :, :] < reach_rows[:, None, None])
    ).astype(jnp.bfloat16)
    extended = jnp.concatenate([pool_before, pool_pre], axis=0).reshape(
        tokens_here + widest, local_groups, group_width
    )
    window_sum = jnp.einsum("gts,sgc->tgc", band, extended, preferred_element_type=jnp.float32)
    global_rows = sp_index * tokens_here + row_ids
    counted = jnp.minimum(global_rows[:, None] + 1, reach_rows[None, :]).astype(jnp.float32)
    own_rows = pool_pre.reshape(tokens_here, local_groups, group_width).astype(jnp.float32)
    pooled = (window_sum / counted[:, :, None] - own_rows).astype(jnp.bfloat16)
    grouped_out = jnp.einsum(
        "tgc,gcd->tgd", pooled, group_weight, preferred_element_type=jnp.float32
    )
    pool_mix = (grouped_out.reshape(tokens_here, local_groups * group_width) * pool_gain).astype(
        jnp.bfloat16
    )
    cell_whole, pool_whole = rows_first((cell_out_weight, pool_out_weight), SP, (1, 1))
    mixed = summed_on_arrival(
        (
            jnp.dot(cell_mix, cell_whole, preferred_element_type=jnp.float32)
            + jnp.dot(pool_mix, pool_whole, preferred_element_type=jnp.float32)
        ).astype(jnp.bfloat16),
        "tp",
        0,
    )
    return mixed.astype(jnp.bfloat16)


def solution(mesh):
    split = Mesh(mesh.devices.reshape(8, 4, 2, mesh.shape["tp"]), ("sp_0", "sp_1", "sp_2", "tp"))
    return jax.shard_map(
        local,
        mesh=split,
        in_specs=(
            P(SP, "tp"),
            P("tp"),
            P(SP, "tp"),
            P(SP, "tp"),
            P(SP, "tp"),
            P(SP, "tp"),
            P(),
            P(),
            P("tp"),
            P(None, "tp"),
            P(None, "tp"),
            P("tp"),
            P(SP, "tp"),
            P("tp", None, None),
            P("tp"),
            P("tp", SP),
            P("tp", SP),
        ),
        out_specs=P(SP_TP, None),
        check_vma=False,
    )
```

profile of v0, /device:TPU:1, one launch (start us, length us, event | category | flops | bytes accessed | tf_op | source)
XLA Modules:
  0.0 364.5 jit_solution(3714666942520899817)
XLA Ops:
  13.7 5.0 %all-to-all-start.1 = ((f32[4,640,1]{1,2,0:T(1,128)}), f32[4,640,1]{1,2,0:T(1,128)S(1)}, u32[]{:S(2)}, u32[]{:S(2)}) async-start(f32[4,640,1]{1,2,0:T(1,128)} %broadcast_in_dim.21), calls=%async_computation.1 | async-start | bytes 20480 | tf_op jit(solution)/shard_map/all_to_all | solution.py:21
  19.0 3.9 %all-to-all-done.1 = f32[4,640,1]{1,2,0:T(1,128)S(1)} async-done(((f32[4,640,1]{1,2,0:T(1,128)}), f32[4,640,1]{1,2,0:T(1,128)S(1)}, u32[]{:S(2)}, u32[]{:S(2)}) %all-to-all-start.1) | async-done | bytes 10272 | tf_op jit(solution)/shard_map/all_to_all | solution.py:21
  22.8 1.8 broadcast_in_dim.20
  24.6 3.8 %all-to-all-start = ((bf16[4,640,512]{1,2,0:T(8,128)(2,1)}), bf16[4,640,512]{1,2,0:T(8,128)(2,1)S(1)}, u32[]{:S(2)}, u32[]{:S(2)}) async-start(bf16[4,640,512]{1,2,0:T(8,128)(2,1)} %broadcast_in_dim.20), calls=%async_computation | async-start | bytes 5242880 | tf_op jit(solution)/shard_map/all_to_all | solution.py:21
  28.5 29.3 %all-to-all-done = bf16[4,640,512]{1,2,0:T(8,128)(2,1)S(1)} async-done(((bf16[4,640,512]{1,2,0:T(8,128)(2,1)}), bf16[4,640,512]{1,2,0:T(8,128)(2,1)S(1)}, u32[]{:S(2)}, u32[]{:S(2)}) %all-to-all-start) | async-done | bytes 2621472 | tf_op jit(solution)/shard_map/all_to_all | solution.py:21
  60.3 1.9 fusion.311
  62.4 37.1 %all-gather.12.cloned.1.call-done = bf16[2048,2304]{1,0:T(8,128)(2,1)} async-done(((bf16[32,2304]{1,0:T(8,128)(2,1)}), bf16[2048,2304]{1,0:T(8,128)(2,1)}) %all-gather.12.cloned.1.call-update) | async-done | bytes 9437200 | tf_op jit(solution)/shard_map/all_gather | solution.py:42
  99.4 2.3 fusion.65
  102.5 3.4 fusion.50
  106.1 3.6 fusion.47
  109.8 2.0 collective-permute-start
  111.8 3.4 fusion.53
  119.4 16.8 %all-gather.16.cloned.1.call-done = f32[2,516,256]{2,1,0:T(8,128)} async-done(((f32[1,516,256]{2,1,0:T(8,128)}), f32[2,516,256]{2,1,0:T(8,128)}) %all-gather.16.cloned.1.call-update) | async-done | bytes 1056784 | tf_op jit(solution)/shard_map/all_gather | solution.py:69
  138.5 1.5 fusion.98
  141.1 33.9 %all-gather.18.cloned.1.call-done = f32[4,516,256]{2,1,0:T(8,128)} async-done(((f32[1,516,256]{2,1,0:T(8,128)}), f32[4,516,256]{2,1,0:T(8,128)}) %all-gather.18.cloned.1.call-update) | async-done | bytes 2113552 | tf_op jit(solution)/shard_map/all_gather | solution.py:69
  177.6 2.0 fusion.91
  187.9 2.3 fusion.3
  190.2 1.9 pad_maximum_fusion.2
  192.2 2.2 multiply_convert_fusion.1
  194.4 3.8 %fusion.76 = f32[2,640,128]{1,2,0:T(8,128)} fusion(bf16[2,128,128]{2,1,0:T(8,128)(2,1)S(1)} %copy-done, bf16[655,2,128]{0,2,1:T(8,128)(2,1)} %bitcast.660, s32[640,655]{0,1:T(8,128)} %iota_subtract_fusion, s32[2]{0:T(128)} %compare_select_fusion.8, pred[640,655]{0,1:T(8,128)(4,1)} %broadcast_compare_fusion, bf16[640,2,128]{0,2,1:T(8,128)(2,1)} %bitcast.659, ...), kind=kOutput, calls=%fused_computation.57 | convolution fusion | flops 258905600 | bytes 3485064 | tf_op jit(solution)/shard_map/tgc,gcd->tgd/dot_general | solution.py:281
  198.2 2.1 fusion.88
  200.3 2.3 fusion.316
  204.2 31.9 %all-gather.20.cloned.1.call-done = f32[8,516,256]{2,1,0:T(8,128)} async-done(((f32[1,516,256]{2,1,0:T(8,128)}), f32[8,516,256]{2,1,0:T(8,128)}) %all-gather.20.cloned.1.call-update) | async-done | bytes 4227088 | tf_op jit(solution)/shard_map/all_gather | solution.py:69
  239.1 1.6 fusion.253
  240.7 2.7 convert_reduce_fusion
  245.6 2.3 fusion.30
  249.4 3.6 fusion.59
  253.0 62.9 %all-gather.14.cloned.1.call-done = bf16[2048,768]{1,0:T(8,128)(2,1)} async-done(((bf16[32,768]{1,0:T(8,128)(2,1)}), bf16[2048,768]{1,0:T(8,128)(2,1)}) %all-gather.14.cloned.1.call-update) | async-done | bytes 3145744 | tf_op jit(solution)/shard_map/all_gather | solution.py:96
  315.9 3.2 fusion.4
  319.0 2.1 add_convert_fusion
  321.2 35.3 %all_to_all.15 = bf16[4,160,2048]{2,1,0:T(8,128)(2,1)S(1)} all-to-all(bf16[4,160,2048]{2,1,0:T(8,128)(2,1)S(1)} %bitcast.633), channel_id=1, replica_groups=mesh['sp_0'=8,'sp_1'=4,'sp_2'=2,'tp'=4] {'tp'}, dimensions={0} | all-to-all | bytes 5242880 | tf_op jit(solution)/shard_map/all_to_all | solution.py:112
  356.4 1.5 reduce_sum.52
  (263 shorter events, 36.8 us)
Async XLA Ops:
  6.5 187.9 %copy-start = (bf16[2,128,128]{2,1,0:T(8,128)(2,1)S(1)}, bf16[2,128,128]{2,1,0:T(8,128)(2,1)}, u32[]{:S(2)}) copy-start(bf16[2,128,128]{2,1,0:T(8,128)(2,1)} %param.30) | copy-start | bytes 196612
  6.5 92.9 %all-gather.12.cloned.1.call-start = ((), (), s32[]{:S(2)}) async-start(), calls=%async_computation.3 | async-start | bytes 9584640 | tf_op jit(solution)/shard_map/all_gather | solution.py:42
  13.7 9.2 %all-to-all-start.1 = ((f32[4,640,1]{1,2,0:T(1,128)}), f32[4,640,1]{1,2,0:T(1,128)S(1)}, u32[]{:S(2)}, u32[]{:S(2)}) async-start(f32[4,640,1]{1,2,0:T(1,128)} %broadcast_in_dim.21), calls=%async_computation.1 | async-start | bytes 20480 | tf_op jit(solution)/shard_map/all_to_all | solution.py:21
  24.6 33.2 %copy-start.70 = (f32[2]{0:T(128)S(1)}, f32[2]{0:T(128)}, u32[]{:S(2)}) copy-start(f32[2]{0:T(128)} %param.25) | copy-start | bytes 28
  24.6 33.2 %all-to-all-start = ((bf16[4,640,512]{1,2,0:T(8,128)(2,1)}), bf16[4,640,512]{1,2,0:T(8,128)(2,1)S(1)}, u32[]{:S(2)}, u32[]{:S(2)}) async-start(bf16[4,640,512]{1,2,0:T(8,128)(2,1)} %broadcast_in_dim.20), calls=%async_computation | async-start | bytes 5242880 | tf_op jit(solution)/shard_map/all_to_all | solution.py:21
  28.4 107.8 %all-gather.16.cloned.1.call-start = ((), (), s32[]{:S(2)}) async-start(), calls=%async_computation.5 | async-start | bytes 1597440 | tf_op jit(solution)/shard_map/all_gather | solution.py:69
  109.8 6.0 %collective-permute-start = (bf16[15,1280]{0,1:T(8,128)(2,1)S(1)}, bf16[15,1280]{0,1:T(8,128)(2,1)S(1)}, u32[]{:S(2)}, u32[]{:S(2)}) collective-permute-start(bf16[15,1280]{0,1:T(8,128)(2,1)S(1)} %pad_maximum_fusion.3), channel_id=1, source_target_pairs={{0,4},{4,8},{8,12},{12,16},{16,20},{20,24},{24,28},{28,32},{32,36}... | collective-permute-start | bytes 115208 | tf_op jit(solution)/shard_map/ppermute | solution.py:52
  119.4 55.7 %all-gather.18.cloned.1.call-start = ((), (), s32[]{:S(2)}) async-start(), calls=%async_computation.6 | async-start | bytes 2662400 | tf_op jit(solution)/shard_map/all_gather | solution.py:69
  140.9 95.2 %all-gather.20.cloned.1.call-start = ((), (), s32[]{:S(2)}) async-start(), calls=%async_computation.7 | async-start | bytes 4792320 | tf_op jit(solution)/shard_map/all_gather | solution.py:69
  180.5 135.3 %all-gather.14.cloned.1.call-start = ((), (), s32[]{:S(2)}) async-start(), calls=%async_computation.4 | async-start | bytes 3194880 | tf_op jit(solution)/shard_map/all_gather | solution.py:96
  202.6 34.5 %copy-start.46 = (f32[2]{0:T(128)S(1)}, f32[2]{0:T(128)}, u32[]{:S(2)}) copy-start(f32[2]{0:T(128)} %copy-done.45) | copy-start | bytes 28
  202.6 34.6 %copy-start.60 = (f32[2]{0:T(128)S(1)}, f32[2]{0:T(128)}, u32[]{:S(2)}) copy-start(f32[2]{0:T(128)} %copy-done.59) | copy-start | bytes 28
  202.6 35.2 %copy-start.40 = (f32[2]{0:T(128)S(1)}, f32[2]{0:T(128)}, u32[]{:S(2)}) copy-start(f32[2]{0:T(128)} %copy-done.39) | copy-start | bytes 28
  202.6 35.2 %copy-start.42 = (f32[2]{0:T(128)S(1)}, f32[2]{0:T(128)}, u32[]{:S(2)}) copy-start(f32[2]{0:T(128)} %copy-done.41) | copy-start | bytes 28
  202.6 35.2 %copy-start.44 = (f32[2]{0:T(128)S(1)}, f32[2]{0:T(128)}, u32[]{:S(2)}) copy-start(f32[2]{0:T(128)} %copy-done.43) | copy-start | bytes 28
  202.6 35.2 %copy-start.54 = (f32[2]{0:T(128)S(1)}, f32[2]{0:T(128)}, u32[]{:S(2)}) copy-start(f32[2]{0:T(128)} %copy-done.53) | copy-start | bytes 28
  202.6 35.2 %copy-start.56 = (f32[2]{0:T(128)S(1)}, f32[2]{0:T(128)}, u32[]{:S(2)}) copy-start(f32[2]{0:T(128)} %copy-done.55) | copy-start | bytes 28
  202.6 35.2 %copy-start.58 = (f32[2]{0:T(128)S(1)}, f32[2]{0:T(128)}, u32[]{:S(2)}) copy-start(f32[2]{0:T(128)} %copy-done.57) | copy-start | bytes 28
  202.6 35.2 %copy-start.21 = (f32[2,640]{1,0:T(2,128)S(1)}, f32[2,640]{1,0:T(2,128)}, u32[]{:S(2)}) copy-start(f32[2,640]{1,0:T(2,128)} %fusion.3) | copy-start | bytes 15364
  202.6 35.3 %copy-start.23 = (f32[2,256]{1,0:T(2,128)S(1)}, f32[2,256]{1,0:T(2,128)}, u32[]{:S(2)}) copy-start(f32[2,256]{1,0:T(2,128)} %copy-done.22) | copy-start | bytes 6148
  202.6 35.3 %copy-start.25 = (f32[2,256]{1,0:T(2,128)S(1)}, f32[2,256]{1,0:T(2,128)}, u32[]{:S(2)}) copy-start(f32[2,256]{1,0:T(2,128)} %copy-done.24) | copy-start | bytes 6148
  202.7 35.3 %copy-start.34 = (f32[2]{0:T(128)S(1)}, f32[2]{0:T(128)}, u32[]{:S(2)}) copy-start(f32[2]{0:T(128)} %copy-done.33) | copy-start | bytes 28
  202.7 35.3 %copy-start.36 = (f32[2]{0:T(128)S(1)}, f32[2]{0:T(128)}, u32[]{:S(2)}) copy-start(f32[2]{0:T(128)} %copy-done.35) | copy-start | bytes 28
  202.7 35.3 %copy-start.38 = (f32[2]{0:T(128)S(1)}, f32[2]{0:T(128)}, u32[]{:S(2)}) copy-start(f32[2]{0:T(128)} %copy-done.37) | copy-start | bytes 28
  202.7 35.3 %copy-start.48 = (f32[2]{0:T(128)S(1)}, f32[2]{0:T(128)}, u32[]{:S(2)}) copy-start(f32[2]{0:T(128)} %copy-done.47) | copy-start | bytes 28
  202.7 35.3 %copy-start.50 = (f32[2]{0:T(128)S(1)}, f32[2]{0:T(128)}, u32[]{:S(2)}) copy-start(f32[2]{0:T(128)} %copy-done.49) | copy-start | bytes 28
  202.7 35.3 %copy-start.52 = (f32[2]{0:T(128)S(1)}, f32[2]{0:T(128)}, u32[]{:S(2)}) copy-start(f32[2]{0:T(128)} %copy-done.51) | copy-start | bytes 28
  202.7 35.3 %copy-start.62 = (f32[2]{0:T(128)S(1)}, f32[2]{0:T(128)}, u32[]{:S(2)}) copy-start(f32[2]{0:T(128)} %copy-done.61) | copy-start | bytes 28
  202.7 35.3 %copy-start.64 = (f32[2]{0:T(128)S(1)}, f32[2]{0:T(128)}, u32[]{:S(2)}) copy-start(f32[2]{0:T(128)} %copy-done.63) | copy-start | bytes 28
  202.7 38.0 %copy-start.18 = (f32[1,2,5,128]{3,1,2,0:T(2,128)S(1)}, f32[1,2,5,128]{3,1,2,0:T(2,128)}, u32[]{:S(2)}) copy-start(f32[1,2,5,128]{3,1,2,0:T(2,128)} %copy-done.17) | copy-start | bytes 15364
  202.7 38.0 %copy-start.20 = (f32[640,2]{0,1:T(2,128)S(1)}, f32[640,2]{0,1:T(2,128)}, u32[]{:S(2)}) copy-start(f32[640,2]{0,1:T(2,128)} %get-tuple-element.107) | copy-start | bytes 15364
  253.0 66.1 %copy-start.3 = (bf16[640,256]{0,1:T(8,128)(2,1)S(1)}, bf16[640,256]{0,1:T(8,128)(2,1)}, u32[]{:S(2)}) copy-start(bf16[640,256]{0,1:T(8,128)(2,1)} %fusion.88) | copy-start | bytes 983044
  (55 other events, 132.6 us)
Sparse Core Ops, SparseCore 0:
  11.1 88.2 all-gather.11
  119.5 16.6 all-gather.15
  141.0 33.9 all-gather.17
  180.6 55.4 all-gather.19
  238.7 77.0 all-gather.13
where the time goes:
time: 366 us; the launch traced here: 364 us
  waiting for transfers between devices  216 us (59%)
  matrix products  36.9 us (10%)
  blocking collectives  35.3 us (10%)
  other arithmetic  30.1 us (8%)
  local copies, waits for them, and re-layouts  20.3 us (6%)
  between operations  14.5 us (4%)
  starting transfers between devices  11.2 us (3%)
    all_gather x3, waiting for transfers between devices, collected_together(): both, at, found = (lax.all_gather(jnp.concatenate(lines), axis), 0, {})  82.5 us
    all_gather x1, waiting for transfers between devices, rows_first(): result, at, done = (lax.all_gather(both, axis, axis=0, tiled=True), 0, [])  62.9 us
    all_gather x1, waiting for transfers between devices, in_one_piece(): result, at, done = (lax.all_gather(both, axis, axis=dim, tiled=True), 0, [])  37.1 us
    all_to_all x1, blocking collectives, summed_on_arrival(): lax.all_to_all(cut_along(array, dim, count), axis, 0, 0, tiled=True)  35.3 us
    all_to_all x2, waiting for transfers between devices, copy_for_each(): return lax.all_to_all(copies, axis, split_axis=0, concat_axis=0, tiled=True)  33.2 us
    dot_general x5, matrix products, local(): jnp.dot(normed, piece_rows, preferred_element_type=jnp.float32)  16.2 us
    all_to_all x2, starting transfers between devices, copy_for_each(): return lax.all_to_all(copies, axis, split_axis=0, concat_axis=0, tiled=True)  8.8 us
    unnamed x179, local copies, waits for them, and re-layouts  7.93 us
  transfers between devices with their start and end apart: 8, of which 8 were waited for; matrix products, arithmetic and copies ran while one was open for 14% of the time, Pallas kernels for 0%

commit v1 on v0

--- a/solution.py
+++ b/solution.py
@@ -1,19 +1,353 @@
+import functools
 import math
 
 import jax
 import jax.numpy as jnp
 from jax import lax
+from jax.experimental import pallas as pl
+from jax.experimental.pallas import tpu as pltpu
 from jax.sharding import Mesh
 from jax.sharding import PartitionSpec as P
 
 LEVELS = 4
-SP = ("sp_0", "sp_1", "sp_2")
-SP_TP = ("sp_0", "sp_1", "sp_2", "tp")
-
-
+NZ, NX, NC, NT = 8, 4, 2, 4
+TOK = 640
+HALO = 32
+ROWS = TOK + HALO
+SP = ("z", "x", "c")
+SP_TP = ("z", "x", "c", "tp")
+MESH = pl.DeviceIdType.MESH
 epsilon = 1e-06
 big_negative = -1e30
+f32 = jnp.float32
+bf16 = jnp.bfloat16
+
+
+class Ring:
+    def __init__(self, send_sems, recv_sems, local_sems):
+        self.send_sems, self.recv_sems, self.local_sems = send_sems, recv_sems, local_sems
+        self.used = 0
+        self.used_local = 0
+        self.pending = []
+
+    def copy(self, src, dst, **where):
+        k = self.used
+        self.used += 1
+        c = pltpu.make_async_remote_copy(
+            src_ref=src,
+            dst_ref=dst,
+            send_sem=self.send_sems.at[k],
+            recv_sem=self.recv_sems.at[k],
+            device_id=where,
+            device_id_type=MESH,
+        )
+        c.start()
+        self.pending.append(c)
+        return c
+
+    def local(self, src, dst):
+        k = self.used_local
+        self.used_local += 1
+        c = pltpu.make_async_copy(src, dst, self.local_sems.at[k])
+        c.start()
+        return c
+
+    def drain(self):
+        for c in self.pending:
+            c.wait_send()
+        self.pending = []
+
+
+def wait_all(copies):
+    for c in copies:
+        c.wait_recv()
+
+
+class Weights:
+    def __init__(self, net, buf, z, x, c):
+        self.net, self.buf, self.z, self.x, self.c = net, buf, z, x, c
+        self.across = {}
+
+    def first(self):
+        net, buf, z, x, c = self.net, self.buf, self.z, self.x, self.c
+        a = buf.at[z, x, c, :, pl.ds(0, 768)]
+        b = buf.at[z, x, c, :, pl.ds(768, 768)]
+        self.a1 = [net.copy(a, a, x=lax.rem(x + d, NX)) for d in (1, 3, 2)]
+        self.b1 = [net.copy(b, b, z=lax.rem(z + d, NZ)) for d in (1, 7, 2, 6, 3, 5, 4)]
+
+    def plane(self, k):
+        return lax.rem(self.z + k + NZ, NZ)
+
+    def share_plane(self, k):
+        part = self.buf.at[self.plane(k), :, self.c, :, pl.ds(0, 768)]
+        self.across["a", k] = self.net.copy(part, part, c=1 - self.c)
+
+    def share_set(self, k):
+        part = self.buf.at[:, lax.rem(self.x + k + NX, NX), self.c, :, pl.ds(768, 768)]
+        self.across["b", k] = self.net.copy(part, part, c=1 - self.c)
+
+    def z_step(self, k):
+        net, buf, z, c = self.net, self.buf, self.z, self.c
+        xs = (pl.ds(0, NX), pl.ds(0, NX)) if k < 4 else (pl.ds(0, 2), pl.ds(2, 2))
+        up = buf.at[self.plane(1 - k), xs[0], c, :, pl.ds(0, 768)]
+        down = buf.at[self.plane(k - 1), xs[1], c, :, pl.ds(0, 768)]
+        self.az = [
+            net.copy(up, up, z=lax.rem(z + 1, NZ)),
+            net.copy(down, down, z=lax.rem(z + NZ - 1, NZ)),
+        ]
+
+    def x_step(self, k):
+        net, buf, x, c = self.net, self.buf, self.x, self.c
+        zs = (pl.ds(0, NZ), pl.ds(0, NZ)) if k < 2 else (pl.ds(0, 4), pl.ds(4, 4))
+        up = buf.at[zs[0], lax.rem(x + NX + 1 - k, NX), c, :, pl.ds(768, 768)]
+        down = buf.at[zs[1], lax.rem(x + k - 1, NX), c, :, pl.ds(768, 768)]
+        self.bx = [
+            net.copy(up, up, x=lax.rem(x + 1, NX)),
+            net.copy(down, down, x=lax.rem(x + NX - 1, NX)),
+        ]
+
+    def a_start(self):
+        wait_all(self.a1)
+        self.z_step(1)
+        self.share_plane(0)
+
+    def b_start(self):
+        wait_all(self.b1)
+        self.x_step(1)
+        self.share_set(0)
+
+    def a_next(self, k):
+        wait_all(self.az)
+        if k < 4:
+            self.z_step(k + 1)
+            self.share_plane(-k)
+            self.share_plane(k)
+        else:
+            self.share_plane(4)
+
+    def b_next(self, k):
+        wait_all(self.bx)
+        if k < 2:
+            self.x_step(k + 1)
+            self.share_set(-1)
+            self.share_set(1)
+        else:
+            self.share_set(2)
+
+    def have(self, *names):
+        for n in names:
+            self.across.pop(n).wait_recv()
+
+
+def enter(z, x, c, t):
+    sp = (z * NX + x) * NC + c
+    n = NZ * NX * NC
+    places = [{"tp": lax.rem(t + d, NT)} for d in range(1, NT)]
+    places += [{"x": lax.rem(x + d, NX)} for d in range(1, NX)]
+    places += [{"z": lax.rem(z + d, NZ)} for d in range(1, NZ)]
+    places += [{"c": 1 - c}]
+    for d in (1, n - 1):
+        places += [{**span_at(lax.rem(sp + d, n)), "tp": k} for k in range(NT)]
+    barrier = pltpu.get_barrier_semaphore()
+    for place in places:
+        pl.semaphore_signal(barrier, inc=1, device_id=place, device_id_type=MESH)
+    pl.semaphore_wait(barrier, len(places))
+
+
+def span_at(sp):
+    return {"z": sp // (NX * NC), "x": lax.rem(sp // NC, NX), "c": lax.rem(sp, NC)}
+
+
+def multiply(rows, planes, buf, acc, base, width, first):
+    def body(n, carry):
+        cols = pl.ds(pl.multiple_of(base + n * 256, 256), 256)
+        for i, k in enumerate(planes):
+            w = buf[k, :, :, :, cols].reshape(NX * NC * 32, 256)
+            part = jnp.dot(rows[k], w, preferred_element_type=f32)
+            if first and i == 0:
+                acc[:, cols] = part
+            else:
+                acc[:, cols] += part
+        return carry
+
+    lax.fori_loop(0, width // 256, body, 0)
+
+
+def gather_inputs_start(net, x_hbm, x_own, X, XH, G, gain, z, x, c, t):
+    sp = (z * NX + x) * NC + c
+    after = span_at(lax.rem(sp + 1, NZ * NX * NC))
+    x_own.wait()
+    up, down = lax.rem(t + 1, NT), lax.rem(t + NT - 1, NT)
+    own = X.at[t]
+    half = TOK // 2
+    top, low = own.at[pl.ds(0, half)], own.at[pl.ds(half, half)]
+    g = [net.copy(gain, G.at[t], tp=lax.rem(t + d, NT)) for d in range(1, NT)]
+    ys = {}
+    ys["u0"] = net.copy(top, top, tp=up)
+    ys["d1"] = net.copy(low, low, tp=down)
+    ys["u1"] = net.copy(low, low, tp=up)
+    ys["d0"] = net.copy(top, top, tp=down)
+    last = own.at[pl.ds(TOK - HALO, HALO)]
+    h = [net.copy(last, XH.at[t], **after, tp=lax.rem(t + d, NT)) for d in range(NT)]
+    return g, ys, h
+
+
+def gather_inputs_forward(net, ys, X, t):
+    up, down = lax.rem(t + 1, NT), lax.rem(t + NT - 1, NT)
+    half = TOK // 2
+    ys["u0"].wait_recv()
+    low_src = X.at[down].at[pl.ds(0, half)]
+    ys["f0"] = net.copy(low_src, low_src, tp=up)
+    ys["d1"].wait_recv()
+    high_src = X.at[up].at[pl.ds(half, half)]
+    ys["f1"] = net.copy(high_src, high_src, tp=down)
+
+
+def scale_block(b, X, G, N, SQ, first):
+    def body(i, carry):
+        r = pl.ds(pl.multiple_of(i * 128, 128), 128)
+        ro = pl.ds(pl.multiple_of(i * 128 + HALO, 32), 128)
+        v = X[b, r, :].astype(f32)
+        n = (v * G[b, 0:1, :]).astype(bf16)
+        N[2 * b, ro, :] = n[:, :256]
+        N[2 * b + 1, ro, :] = n[:, 256:]
+        s = v * v
+        s = s[:, 0:128] + s[:, 128:256] + s[:, 256:384] + s[:, 384:512]
+        SQ[ro, :] = s if first else SQ[ro, :] + s
+        return carry
+
+    lax.fori_loop(0, TOK // 128, body, 0)
+
+
+def scale_halo(XH, G, N, SQ, sp):
+    total = None
+    for b in range(NT):
+        v = jnp.where(sp > 0, XH[b].astype(f32), 0.0)
+        n = (v * G[b, 0:1, :]).astype(bf16)
+        N[2 * b, 0:HALO, :] = n[:, :256]
+        N[2 * b + 1, 0:HALO, :] = n[:, 256:]
+        s = v * v
+        s = s[:, 0:128] + s[:, 128:256] + s[:, 256:384] + s[:, 384:512]
+        total = s if total is None else total + s
+    SQ[0:HALO, :] = total
 highest = lax.Precision.HIGHEST
+
+
+def gather_and_project(
+    x_hbm, gain, wq, wk, wv, wo, wp, wout, ig, fg,
+    qkv_out, gate_out, keep_out, og_out, wout_out,
+    X, XH, G, N, SQ, INV, W1, W2, A1, A2, send_sems, recv_sems, local_sems,
+):
+    z, x, c, t = (lax.axis_index(n) for n in SP_TP)
+    sp = (z * NX + x) * NC + c
+    net = Ring(send_sems, recv_sems, local_sems)
+    x_own = net.local(x_hbm, X.at[t])
+    mine1, mine2 = W1.at[z, x, c], W2.at[z, x, c]
+    load1 = [net.local(w, mine1.at[:, pl.ds(512 * i, 512)]) for i, w in enumerate((wq, wk, wv))]
+    load2 = [
+        net.local(wo, mine2.at[:, pl.ds(0, 512)]),
+        net.local(wp, mine2.at[:, pl.ds(512, 256)]),
+        net.local(wout, mine2.at[:, pl.ds(768, 768)]),
+    ]
+    enter(z, x, c, t)
+    for l in load1:
+        l.wait()
+    w1 = Weights(net, W1, z, x, c)
+    w2 = Weights(net, W2, z, x, c)
+    w1.first()
+    g, ys, h = gather_inputs_start(net, x_hbm, x_own, X, XH, G, gain, z, x, c, t)
+    G[t] = gain[...]
+    scale_block(t, X, G, N, SQ, True)
+    w1.a_start()
+    gather_inputs_forward(net, ys, X, t)
+    w1.b_start()
+    for l in load2:
+        l.wait()
+    w1.a_next(1)
+    w2.first()
+    wait_all(g)
+    ys["u1"].wait_recv()
+    ys["d0"].wait_recv()
+    scale_block(lax.rem(t + NT - 1, NT), X, G, N, SQ, False)
+    w1.b_next(1)
+    scale_block(lax.rem(t + 1, NT), X, G, N, SQ, False)
+    w1.a_next(2)
+    w2.a_start()
+    w2.b_start()
+    ys["f0"].wait_recv()
+    ys["f1"].wait_recv()
+    scale_block(lax.rem(t + 2, NT), X, G, N, SQ, False)
+    wait_all(h)
+    scale_halo(XH, G, N, SQ, sp)
+    INV[...] = lax.rsqrt(jnp.sum(SQ[...], axis=1, keepdims=True) / (NT * 512) + epsilon)
+    gates = jnp.zeros((TOK, 8), f32)
+    keeps = jnp.zeros((TOK, 8), f32)
+    for k in range(NZ):
+        rows = N[k, HALO:, :]
+        gates += jnp.dot(rows, ig[k * 256 : (k + 1) * 256, :], preferred_element_type=f32)
+        keeps += jnp.dot(rows, fg[k * 256 : (k + 1) * 256, :], preferred_element_type=f32)
+    gate_out[...] = gates * INV[HALO:, :]
+    keep_out[...] = keeps * INV[HALO:, :]
+    w1.a_next(3)
+    w1.b_next(2)
+    w1.have(("a", 0), ("a", -1), ("a", 1), ("a", -2), ("a", 2))
+    w2.a_next(1)
+    multiply(N, [w1.plane(k) for k in (0, -1, 1, -2, 2)], W1, A1, 0, 768, True)
+    w1.a_next(4)
+    w2.b_next(1)
+    w1.have(("a", -3), ("a", 3))
+    multiply(N, [w1.plane(k) for k in (-3, 3)], W1, A1, 0, 768, False)
+    w1.have(("b", 0), ("b", -1), ("b", 1), ("b", 2))
+    multiply(N, list(range(NZ)), W1, A1, 768, 768, True)
+    w1.have(("a", 4))
+    multiply(N, [w1.plane(4)], W1, A1, 0, 768, False)
+    qkv_out[...] = (A1[...] * INV[...]).astype(bf16)
+    w2.a_next(2)
+    w2.b_next(2)
+    w2.a_next(3)
+    w2.a_next(4)
+    w2.have(*[("a", k) for k in (0, -1, 1, -2, 2, -3, 3, 4)])
+    multiply(N, list(range(NZ)), W2, A2, 0, 768, True)
+    og_out[...] = (A2[...] * INV[...]).astype(bf16)
+    w2.have(*[("b", k) for k in (0, -1, 1, 2)])
+    wout_out[...] = W2[:, :, :, :, 768:].reshape(2048, 768)
+    net.drain()
+
+
+def projections(inputs, gain, weights, wout, ig, fg):
+    hbm = pl.BlockSpec(memory_space=pl.ANY)
+    vmem = pl.BlockSpec(memory_space=pltpu.VMEM)
+    return pl.pallas_call(
+        gather_and_project,
+        out_shape=(
+            jax.ShapeDtypeStruct((ROWS, 1536), bf16),
+            jax.ShapeDtypeStruct((TOK, 8), f32),
+            jax.ShapeDtypeStruct((TOK, 8), f32),
+            jax.ShapeDtypeStruct((ROWS, 768), bf16),
+            jax.ShapeDtypeStruct((2048, 768), bf16),
+        ),
+        in_specs=[hbm, vmem] + [hbm] * 6 + [vmem] * 2,
+        out_specs=(vmem,) * 5,
+        scratch_shapes=[
+            pltpu.VMEM((NT, TOK, 512), bf16),
+            pltpu.VMEM((NT, HALO, 512), bf16),
+            pltpu.VMEM((NT, 8, 512), f32),
+            pltpu.VMEM((NZ, ROWS, 256), bf16),
+            pltpu.VMEM((ROWS, 128), f32),
+            pltpu.VMEM((ROWS, 1), f32),
+            pltpu.VMEM((NZ, NX, NC, 32, 1536), bf16),
+            pltpu.VMEM((NZ, NX, NC, 32, 1536), bf16),
+            pltpu.VMEM((ROWS, 1536), f32),
+            pltpu.VMEM((ROWS, 768), f32),
+            pltpu.SemaphoreType.DMA((96,)),
+            pltpu.SemaphoreType.DMA((96,)),
+            pltpu.SemaphoreType.DMA((8,)),
+        ],
+        compiler_params=pltpu.CompilerParams(
+            collective_id=0, has_side_effects=True, vmem_limit_bytes=60 * 2**20
+        ),
+        name="gather_and_project",
+    )(inputs, gain, *weights, wout, ig, fg)
 
 
 def copy_for_each(array, axis):
@@ -180,38 +514,32 @@
     cell_out_weight,
     pool_out_weight,
 ):
-    local_wide = inputs.astype(jnp.float32)
-    squares = taken_together(jnp.sum(local_wide * local_wide, axis=1, keepdims=True), "tp")
-    normed = gather_directly(
-        (local_wide * norm_gain.astype(jnp.float32)).astype(jnp.bfloat16), "tp", 1
-    )
-    inverse_rms = lax.rsqrt(squares / normed.shape[1] + epsilon)
-    pieces = in_one_piece(
-        (query_weight, key_weight, value_weight, outgate_weight, pool_weight), SP, 0, 1
-    )
-    products = tuple(
-        (jnp.dot(normed, piece_rows, preferred_element_type=jnp.float32) for piece_rows in pieces)
-    )
-    query_pre, key_pre, value_rows, outgate_pre, pool_pre = tuple(
-        ((product * inverse_rms).astype(jnp.bfloat16) for product in products)
+    gain = jnp.broadcast_to(norm_gain.astype(f32)[None, :], (8, 512))
+    wout = jnp.concatenate([cell_out_weight, pool_out_weight], axis=0).T
+    qkv, log_in_all, keep_all, ogp, wout_all = projections(
+        inputs,
+        gain,
+        (query_weight, key_weight, value_weight, outgate_weight, pool_weight),
+        wout,
+        inputgate_weight,
+        forget_weight,
     )
     tp_index = lax.axis_index("tp")
     sp_index = lax.axis_index(SP)
     tokens_here = inputs.shape[0]
     sequence_log = math.log(tokens_here * lax.axis_size(SP))
     local_heads = forget_bias.shape[0]
-    gate_cols = lax.dynamic_slice_in_dim(inputgate_weight, tp_index * local_heads, local_heads, 1)
-    keep_cols = lax.dynamic_slice_in_dim(forget_weight, tp_index * local_heads, local_heads, 1)
-    log_in = jnp.dot(normed, gate_cols, preferred_element_type=jnp.float32) * inverse_rms
+    log_in = lax.dynamic_slice_in_dim(log_in_all, tp_index * local_heads, local_heads, 1)
     log_keep = jax.nn.log_sigmoid(
-        jnp.dot(normed, keep_cols, preferred_element_type=jnp.float32) * inverse_rms
+        lax.dynamic_slice_in_dim(keep_all, tp_index * local_heads, local_heads, 1)
         + forget_bias
         + sequence_log
     )
     widest = 2**LEVELS - 1
-    query_width = query_pre.shape[1]
-    edges = jnp.concatenate([query_pre[-widest:], key_pre[-widest:], pool_pre[-widest:]], axis=1)
-    before = shifted(edges, SP, 1)
+    query_width = 512
+    before = jnp.concatenate([qkv[HALO - widest : HALO, :1024], ogp[HALO - widest : HALO, 512:]], axis=1)
+    query_pre, key_pre, value_rows = (qkv[HALO:, 512 * i : 512 * (i + 1)] for i in range(3))
+    outgate_pre, pool_pre = ogp[HALO:, :512], ogp[HALO:, 512:]
     margin = conv_query.shape[0] - 1
     query_taps = causal_taps(
         jnp.concatenate([before[widest - margin :, :query_width], query_pre], axis=0), conv_query
@@ -284,11 +612,12 @@
     pool_mix = (grouped_out.reshape(tokens_here, local_groups * group_width) * pool_gain).astype(
         jnp.bfloat16
     )
-    cell_whole, pool_whole = rows_first((cell_out_weight, pool_out_weight), SP, (1, 1))
     mixed = summed_on_arrival(
-        (
-            jnp.dot(cell_mix, cell_whole, preferred_element_type=jnp.float32)
-            + jnp.dot(pool_mix, pool_whole, preferred_element_type=jnp.float32)
+        lax.dot_general(
+            jnp.concatenate([cell_mix, pool_mix], axis=1),
+            wout_all,
+            (((1,), (1,)), ((), ())),
+            preferred_element_type=jnp.float32,
         ).astype(jnp.bfloat16),
         "tp",
         0,
@@ -297,7 +626,7 @@
 
 
 def solution(mesh):
-    split = Mesh(mesh.devices.reshape(8, 4, 2, mesh.shape["tp"]), ("sp_0", "sp_1", "sp_2", "tp"))
+    split = Mesh(mesh.devices.reshape(8, 4, 2, mesh.shape["tp"]), SP_TP)
     return jax.shard_map(
         local,
         mesh=split,

time: 366 us -> 280 us (0.77)
  waiting for transfers between devices: 216 us -> 84.7 us
  Pallas kernels: 0 us -> 77 us
  matrix products: 36.9 us -> 16.5 us
  starting transfers between devices: 11.2 us -> 0.27 us
  other arithmetic: 30.1 us -> 22.6 us
  local copies, waits for them, and re-layouts: 20.3 us -> 27.6 us
    all_gather x2 -> x0, waiting for transfers between devices: 99.9 us -> none  [the longest x1 62.9 us: rows_first(): result, at, done = (lax.all_gather(both, axis, axis=0, tiled=True), 0, [])]
    pallas_call x0 -> x1, Pallas kernels: none -> 77 us  [projections(): pl.pallas_call(gather_and_project, out_shape=(jax.ShapeDtypeStruct((ROWS,...]
    all_to_all x2 -> x0, waiting for transfers between devices: 33.2 us -> none  [copy_for_each(): return lax.all_to_all(copies, axis, split_axis=0, concat_axis=0, tiled=True)]
    dot_general x9 -> x1, matrix products: 24.7 us -> 4.12 us  [local(): lax.dot_general(jnp.concatenate([cell_mix, pool_mix], axis=1), wout_all,...]
    all_to_all x2 -> x0, starting transfers between devices: 8.8 us -> none  [copy_for_each(): return lax.all_to_all(copies, axis, split_axis=0, concat_axis=0, tiled=True)]
    reshape x1 -> x5, local copies, waits for them, and re-layouts: 0.01 us -> 5.21 us  [the longest x1 2.16 us: local(): grouped_out.reshape(tokens_here, local_groups * group_width) * pool_gain]
    unnamed x179 -> x199, local copies, waits for them, and re-layouts: 7.93 us -> 7.2 us
  transfers between devices with their start and end apart: 8 -> 3, of which waited for: 8 -> 3; matrix products, arithmetic and copies ran while one was open for 14% -> 5% of each run, Pallas kernels for 0% -> 0%
where the time goes in v1:
time: 280 us; the launch traced here: 279 us
  waiting for transfers between devices  84.7 us (30%)
  Pallas kernels  77 us (28%)
  blocking collectives  35.4 us (13%)
  local copies, waits for them, and re-layouts  27.6 us (10%)
  other arithmetic  22.6 us (8%)
  matrix products  16.5 us (6%)
  between operations  14.8 us (5%)
    all_gather x3, waiting for transfers between devices, collected_together(): both, at, found = (lax.all_gather(jnp.concatenate(lines), axis), 0, {})  84.7 us
    pallas_call x1, Pallas kernels, projections(): pl.pallas_call(gather_and_project, out_shape=(jax.ShapeDtypeStruct((ROWS,...  77 us
    all_to_all x1, blocking collectives, summed_on_arrival(): lax.all_to_all(cut_along(array, dim, count), axis, 0, 0, tiled=True)  35.4 us
    unnamed x199, local copies, waits for them, and re-layouts  7.2 us
    slice x3, local copies, waits for them, and re-layouts, carried_in(): subtotal = combine(subtotal, jax.tree.map(lambda part: part[k], pieces))  6.4 us
  transfers between devices with their start and end apart: 3, of which 3 were waited for; matrix products, arithmetic and copies ran while one was open for 5% of the time, Pallas kernels for 0%

profile of v1, /device:TPU:1, one launch (start us, length us, event | category | flops | bytes accessed | tf_op | source)
XLA Modules:
  0.0 278.9 jit_solution(16955039375060989301)
XLA Ops:
  6.5 1.8 copy.104.ig
  8.3 1.8 copy.105.fg
  10.1 1.4 maximum_bitcast_fusion.3.wout
  11.5 1.3 broadcast_in_dim.18.gain
  12.8 77.0 %gather_and_project.1 = (bf16[672,1536]{1,0:T(8,128)(2,1)}, f32[640,8]{1,0:T(8,128)}, f32[640,8]{1,0:T(8,128)}, bf16[672,768]{1,0:T(8,128)(2,1)}, bf16[2048,768]{1,0:T(8,128)(2,1)}) custom-call(bf16[640,512]{1,0:T(8,128)(2,1)} %x_hbm.1, f32[8,512]{1,0:T(8,128)} %broadcast_in_dim.18.gain, bf16[32,512]{1,0:T(8,128)(2,1)} %wq.1, bf16[32,512]{1,0:T(8,128)(2,1)} %wk.1, ...), custom_call_target="tpu_custom_call" | custom-call | tf_op jit(solution)/shard_map/gather_and_project/pallas_call | solution.py:320
  89.8 1.3 fusion.117
  94.6 0.9 slice.351
  95.5 2.6 multiply_convert_fusion.3
  98.4 1.4 copy.142
  101.4 11.7 %all-gather.10.cloned.1.call-done = f32[2,516,256]{2,1,0:T(8,128)} async-done(((f32[1,516,256]{2,1,0:T(8,128)}), f32[2,516,256]{2,1,0:T(8,128)}) %all-gather.10.cloned.1.call-update) | async-done | bytes 1056784 | tf_op jit(solution)/shard_map/all_gather | solution.py:403
  115.4 1.5 fusion.45
  118.1 33.9 %all-gather.12.cloned.1.call-done = f32[4,516,256]{2,1,0:T(8,128)} async-done(((f32[1,516,256]{2,1,0:T(8,128)}), f32[4,516,256]{2,1,0:T(8,128)}) %all-gather.12.cloned.1.call-update) | async-done | bytes 2113552 | tf_op jit(solution)/shard_map/all_gather | solution.py:403
  154.4 2.0 fusion.38
  156.4 0.9 maximum_bitcast_fusion.2
  157.9 1.1 copy.140
  159.0 1.1 reshape.2694
  160.7 3.3 %fusion.23 = f32[2,640,128]{1,2,0:T(8,128)} fusion(bf16[2,128,128]{2,1,0:T(8,128)(2,1)S(1)} %copy-done, f32[640,2,128]{0,2,1:T(8,128)} %bitcast.627, s32[640,655]{0,1:T(8,128)S(1)} %iota_subtract_fusion, s32[2]{0:T(128)S(1)} %compare_select_fusion.8, pred[640,655]{0,1:T(8,128)(4,1)S(1)} %broadcast_compare_fusion, bf16[655,2,128]{2,1,0:T(2,128)(2,1)} %reshape.2694, ...), kind=kOutput, calls=%fused_computation.27 | convolution fusion | flops 258741760 | bytes 3812744 | tf_op jit(solution)/shard_map/tgc,gcd->tgd/dot_general | solution.py:609
  163.9 2.2 copy.141
  168.1 2.0 multiply_convert_fusion.6
  170.2 2.3 fusion.263
  172.4 1.4 fusion.261
  173.8 39.1 %all-gather.14.cloned.1.call-done = f32[8,516,256]{2,1,0:T(8,128)} async-done(((f32[1,516,256]{2,1,0:T(8,128)}), f32[8,516,256]{2,1,0:T(8,128)}) %all-gather.14.cloned.1.call-update) | async-done | bytes 4227088 | tf_op jit(solution)/shard_map/all_gather | solution.py:403
  212.8 0.9 fusion.260
  214.8 1.0 fusion.204
  216.0 1.7 fusion.30
  218.1 3.7 %convert_reduce_fusion = (f32[2,640]{1,0:T(2,128)S(1)}, bf16[2,640,640]{1,2,0:T(8,128)(2,1)}) fusion(f32[2,640]{1,0:T(2,128)S(1)} %copy.121, f32[2,640]{1,0:T(2,128)S(1)} %copy.115, f32[2,640]{1,0:T(2,128)S(1)} %copy.113, pred[640,640]{0,1:T(8,128)(4,1)} %copy-done.4, bf16[80,2,8,256]{3,2,1,0:T(8,128)(2,1)S(1)} %bitcast.620, ...), kind=kOutput, calls=%fused_computation.3 | convolution fusion | flops 425982720 | bytes 3379200 | tf_op jit(solution)/shard_map/thd,shd->hts/dot_general | solution.py:483
  222.8 2.8 fusion.259
  226.0 2.2 fusion.8
  229.9 1.5 multiply_convert_fusion.1
  231.4 4.1 %convolution_convert_fusion = bf16[640,2048]{1,0:T(8,128)(2,1)S(1)} fusion(bf16[2048,768]{1,0:T(8,128)(2,1)} %get-tuple-element.14, bf16[640,256]{1,0:T(8,128)(2,1)S(1)} %copy-done.15, bf16[640,512]{1,0:T(8,128)(2,1)S(1)} %multiply_convert_fusion.1), kind=kOutput, calls=%fused_computation.7 | convolution fusion | flops 2016542720 | bytes 6750208 | tf_op jit(solution)/shard_map/dot_general | solution.py:616
  235.5 35.4 %all_to_all.5 = bf16[4,160,2048]{2,1,0:T(8,128)(2,1)S(1)} all-to-all(bf16[4,160,2048]{2,1,0:T(8,128)(2,1)S(1)} %bitcast.617), channel_id=1, replica_groups=mesh['z'=8,'x'=4,'c'=2,'tp'=4] {'tp'}, dimensions={0} | all-to-all | bytes 5242880 | tf_op jit(solution)/shard_map/all_to_all | solution.py:446
  270.9 1.5 reduce_sum.32
  (268 shorter events, 17.6 us)
Async XLA Ops:
  6.5 154.1 %copy-start = (bf16[2,128,128]{2,1,0:T(8,128)(2,1)S(1)}, bf16[2,128,128]{2,1,0:T(8,128)(2,1)}, u32[]{:S(2)}) copy-start(bf16[2,128,128]{2,1,0:T(8,128)(2,1)} %param.30) | copy-start | bytes 196612
  6.5 106.6 %all-gather.10.cloned.1.call-start = ((), (), s32[]{:S(2)}) async-start(), calls=%async_computation.1 | async-start | bytes 1597440 | tf_op jit(solution)/shard_map/all_gather | solution.py:403
  8.3 81.4 %copy-start.84 = (f32[2]{0:T(128)S(1)}, f32[2]{0:T(128)}, u32[]{:S(2)}) copy-start(f32[2]{0:T(128)} %param.25) | copy-start | bytes 28
  89.8 3.3 %copy-start.5 = (f32[640,8]{1,0:T(8,128)S(1)}, f32[640,8]{1,0:T(8,128)}, u32[]{:S(2)}) copy-start(f32[640,8]{1,0:T(8,128)} %get-tuple-element.12) | copy-start | bytes 61444
  101.3 50.6 %all-gather.12.cloned.1.call-start = ((), (), s32[]{:S(2)}) async-start(), calls=%async_computation.2 | async-start | bytes 2662400 | tf_op jit(solution)/shard_map/all_gather | solution.py:403
  114.0 3.8 %copy-start.31 = (f32[2]{0:T(128)}, f32[2]{0:T(128)S(1)}, u32[]{:S(2)}) copy-start(f32[2]{0:T(128)S(1)} %get-tuple-element.94) | copy-start | bytes 28
  117.8 95.0 %all-gather.14.cloned.1.call-start = ((), (), s32[]{:S(2)}) async-start(), calls=%async_computation.3 | async-start | bytes 4792320 | tf_op jit(solution)/shard_map/all_gather | solution.py:403
  152.9 3.4 %copy-start.37 = (f32[2]{0:T(128)}, f32[2]{0:T(128)S(1)}, u32[]{:S(2)}) copy-start(f32[2]{0:T(128)S(1)} %get-tuple-element.36) | copy-start | bytes 28
  153.0 3.4 %copy-start.85 = (f32[2]{0:T(128)}, f32[2]{0:T(128)S(1)}, u32[]{:S(2)}) copy-start(f32[2]{0:T(128)S(1)} %subtract_exponential_fusion.21) | copy-start | bytes 28
  168.1 4.3 %copy-start.2 = (f32[4,516,256]{2,1,0:T(8,128)S(1)}, f32[4,516,256]{2,1,0:T(8,128)}, u32[]{:S(2)}) copy-start(f32[4,516,256]{2,1,0:T(8,128)} %all-gather.12.cloned.1.call-done) | copy-start | bytes 6340612
  222.5 3.3 %copy-start.14 = (f32[1,512,256]{2,1,0:T(8,128)S(1)}, f32[1,512,256]{2,1,0:T(8,128)}, u32[]{:S(2)}) copy-start(f32[1,512,256]{2,1,0:T(8,128)} %get-tuple-element.55) | copy-start | bytes 1572868
  222.5 3.3 %copy-start.22 = (f32[2]{0:T(128)S(1)}, f32[2]{0:T(128)}, u32[]{:S(2)}) copy-start(f32[2]{0:T(128)} %copy-done.21) | copy-start | bytes 28
  222.5 3.2 %copy-start.24 = (f32[2]{0:T(128)S(1)}, f32[2]{0:T(128)}, u32[]{:S(2)}) copy-start(f32[2]{0:T(128)} %copy-done.23) | copy-start | bytes 28
  222.5 3.2 %copy-start.26 = (f32[2]{0:T(128)S(1)}, f32[2]{0:T(128)}, u32[]{:S(2)}) copy-start(f32[2]{0:T(128)} %copy-done.25) | copy-start | bytes 28
  222.5 3.2 %copy-start.32 = (f32[2]{0:T(128)S(1)}, f32[2]{0:T(128)}, u32[]{:S(2)}) copy-start(f32[2]{0:T(128)} %copy-done.31) | copy-start | bytes 28
  222.5 3.2 %copy-start.34 = (f32[2]{0:T(128)S(1)}, f32[2]{0:T(128)}, u32[]{:S(2)}) copy-start(f32[2]{0:T(128)} %copy-done.33) | copy-start | bytes 28
  222.5 3.2 %copy-start.38 = (f32[2]{0:T(128)S(1)}, f32[2]{0:T(128)}, u32[]{:S(2)}) copy-start(f32[2]{0:T(128)} %copy-done.37) | copy-start | bytes 28
  222.5 3.2 %copy-start.40 = (f32[2]{0:T(128)S(1)}, f32[2]{0:T(128)}, u32[]{:S(2)}) copy-start(f32[2]{0:T(128)} %copy-done.39) | copy-start | bytes 28
  222.5 3.2 %copy-start.42 = (f32[2]{0:T(128)S(1)}, f32[2]{0:T(128)}, u32[]{:S(2)}) copy-start(f32[2]{0:T(128)} %copy-done.41) | copy-start | bytes 28
  222.6 3.2 %copy-start.44 = (f32[2]{0:T(128)S(1)}, f32[2]{0:T(128)}, u32[]{:S(2)}) copy-start(f32[2]{0:T(128)} %copy-done.43) | copy-start | bytes 28
  222.6 3.2 %copy-start.46 = (f32[2]{0:T(128)S(1)}, f32[2]{0:T(128)}, u32[]{:S(2)}) copy-start(f32[2]{0:T(128)} %copy-done.45) | copy-start | bytes 28
  222.6 3.2 %copy-start.48 = (f32[2]{0:T(128)S(1)}, f32[2]{0:T(128)}, u32[]{:S(2)}) copy-start(f32[2]{0:T(128)} %copy-done.47) | copy-start | bytes 28
  222.6 3.2 %copy-start.50 = (f32[2]{0:T(128)S(1)}, f32[2]{0:T(128)}, u32[]{:S(2)}) copy-start(f32[2]{0:T(128)} %copy-done.49) | copy-start | bytes 28
  222.6 3.2 %copy-start.52 = (f32[2]{0:T(128)S(1)}, f32[2]{0:T(128)}, u32[]{:S(2)}) copy-start(f32[2]{0:T(128)} %copy-done.51) | copy-start | bytes 28
  222.6 3.2 %copy-start.54 = (f32[2]{0:T(128)S(1)}, f32[2]{0:T(128)}, u32[]{:S(2)}) copy-start(f32[2]{0:T(128)} %copy-done.53) | copy-start | bytes 28
  222.6 3.2 %copy-start.56 = (f32[2]{0:T(128)S(1)}, f32[2]{0:T(128)}, u32[]{:S(2)}) copy-start(f32[2]{0:T(128)} %copy-done.55) | copy-start | bytes 28
  222.6 3.2 %copy-start.58 = (f32[2]{0:T(128)S(1)}, f32[2]{0:T(128)}, u32[]{:S(2)}) copy-start(f32[2]{0:T(128)} %copy-done.57) | copy-start | bytes 28
  222.6 3.2 %copy-start.60 = (f32[2]{0:T(128)S(1)}, f32[2]{0:T(128)}, u32[]{:S(2)}) copy-start(f32[2]{0:T(128)} %copy-done.59) | copy-start | bytes 28
  222.6 3.2 %copy-start.62 = (f32[2]{0:T(128)S(1)}, f32[2]{0:T(128)}, u32[]{:S(2)}) copy-start(f32[2]{0:T(128)} %copy-done.61) | copy-start | bytes 28
  222.7 3.2 %copy-start.64 = (f32[2]{0:T(128)S(1)}, f32[2]{0:T(128)}, u32[]{:S(2)}) copy-start(f32[2]{0:T(128)} %copy-done.63) | copy-start | bytes 28
  222.7 3.2 %copy-start.66 = (f32[2]{0:T(128)S(1)}, f32[2]{0:T(128)}, u32[]{:S(2)}) copy-start(f32[2]{0:T(128)} %copy-done.65) | copy-start | bytes 28
  222.7 3.2 %copy-start.68 = (f32[2]{0:T(128)S(1)}, f32[2]{0:T(128)}, u32[]{:S(2)}) copy-start(f32[2]{0:T(128)} %copy-done.67) | copy-start | bytes 28
  (61 other events, 117.6 us)
Sparse Core Ops, SparseCore 0:
  101.5 11.6 all-gather.9
  117.9 33.9 all-gather.11
  157.4 55.4 all-gather.13
